TPU v7x, 32 devices: a whole 2x2x4 slice. The times are simulated.
32 devices in a mesh: tp: 8 (over z, y), dp: 4 (over x, core).
Axes of the slice: x: 2, y: 2, z: 4, core: 2. Of those that a mesh axis runs over, the one named last changes fastest.
Arguments:
- tokens: bfloat16 [128, 4096], P('dp', 'tp'), may hold values from -6 to 6
- lengths: int32 [128], P('dp'), may hold values from 1 to 96, 3072 in all
- norm_gain: float32 [2, 4096], replicated, may hold values from 0.1 to 1.9
- w_recept: bfloat16 [2, 4096, 4096], P(None, None, ('tp', 'dp')), may hold values from -0.09375 to 0.09375
- w_key: bfloat16 [2, 4096, 4096], P(None, None, ('tp', 'dp')), may hold values from -0.09375 to 0.09375
- w_value: bfloat16 [2, 4096, 4096], P(None, None, ('tp', 'dp')), may hold values from -0.09375 to 0.09375
- w_decay: bfloat16 [2, 4096, 4096], P(None, None, ('tp', 'dp')), may hold values from -0.09375 to 0.09375
- w_rate: bfloat16 [2, 4096, 4096], P(None, None, ('tp', 'dp')), may hold values from -0.09375 to 0.09375
- w_gate: bfloat16 [2, 4096, 4096], P(None, None, ('tp', 'dp')), may hold values from -0.09375 to 0.09375
- w_out: bfloat16 [2, 4096, 4096], P(None, None, ('tp', 'dp')), may hold values from -0.09375 to 0.09375
- decay_base: float32 [2, 4096], P(None, 'tp'), may hold values from -3 to 1
- rate_base: float32 [2, 4096], P(None, 'tp'), may hold values from -3 to 3
- group_gain: float32 [2, 4096], P(None, 'tp'), may hold values from 0.1 to 1.9
- state: float32 [2, 128, 64, 64, 64], P(None, 'dp', 'tp'), may hold values from -6 to 6
Outputs:
- mixed: bfloat16 [128, 4096], P('dp', 'tp')
- new_state: float32 [2, 128, 64, 64, 64], P(None, 'dp', 'tp')
Inputs may be any that keep to these rules, and one draw needn't show every extreme that they name: Each sequence's live length lies between 1 and 96, some sequences reach 96, and the lengths sum to 3072.
All inputs are finite; a program needn't handle non-finite values.
Results may differ from a plain program's by a relative error of at most 0.025.
Values may be sent and summed in bfloat16 or wider, within the bound.
A program may use at most 128 MiB of HBM per device.

v0:
```python
import jax
import jax.numpy as jnp
from jax import lax
from jax.sharding import PartitionSpec as P

STEP = 16


RMS_EPS = 1e-06
GROUP_EPS = 0.00064


def as_sent(value):
    def short(part):
        return part.astype(jnp.bfloat16) if part.dtype == jnp.float32 else part

    return jax.tree.map(short, value)


def taken_in(section, axis, dim, hop, start):
    def gathered(part):
        return lax.all_gather(part, axis, axis=dim, tiled=True)

    return hop(start, jax.tree.map(gathered, section), jnp.int32(0))


def recur(state_old, recept, key_vec, value_vec, decay_rate, learn_rate, active, head_size):
    split = (recept.shape[0], -1, head_size)
    recept_h = recept.reshape(split)
    key_h = key_vec.reshape(split)
    value_h = value_vec.reshape(split)
    decay_h = decay_rate.reshape(split)
    rate_h = learn_rate.reshape(split)
    key_len = jnp.sqrt(jnp.sum(key_h * key_h, axis=-1, keepdims=True))
    key_unit = key_h / jnp.maximum(key_len, 1e-12)
    state_a = jnp.einsum("bhij,bhj->bhi", state_old, -key_unit, precision=lax.Precision.HIGHEST)
    updated = (
        state_old * decay_h[:, :, None, :]
        + state_a[:, :, :, None] * (key_unit * rate_h)[:, :, None, :]
        + value_h[:, :, :, None] * (key_h * rate_h)[:, :, None, :]
    )
    updated = jnp.where(active[:, None, None, None], updated, state_old)
    readout = jnp.einsum("bhij,bhj->bhi", updated, recept_h, precision=lax.Precision.HIGHEST)
    centre = jnp.mean(readout, axis=-1, keepdims=True)
    spread = jnp.mean(jnp.square(readout - centre), axis=-1, keepdims=True)
    normal_out = ((readout - centre) * lax.rsqrt(spread + GROUP_EPS)).reshape(recept.shape[0], -1)
    return (updated, normal_out)


def on_device(
    tokens,
    lengths,
    norm_gain,
    w_recept,
    w_key,
    w_value,
    w_decay,
    w_rate,
    w_gate,
    w_out,
    decay_base,
    rate_base,
    group_gain,
    state,
):
    slim = w_recept.shape[2]
    head_size = state.shape[-1]
    active = lengths > STEP
    current = tokens
    updated_states = []
    for layer_idx in range(2):
        joined = jnp.concatenate(
            [
                w_recept[layer_idx],
                w_key[layer_idx],
                w_value[layer_idx],
                w_decay[layer_idx],
                w_rate[layer_idx],
                w_gate[layer_idx],
            ],
            axis=1,
        )
        batch_raw = lax.all_gather(current, "dp", axis=0, tiled=True)
        every_feature = lax.all_gather(batch_raw, "tp", axis=1, tiled=True)
        values = every_feature.astype(jnp.float32)
        factor = lax.rsqrt(jnp.mean(values * values, axis=1, keepdims=True) + RMS_EPS)
        normed = (values * factor * norm_gain[layer_idx]).astype(jnp.bfloat16)
        projected = jnp.dot(normed, joined, preferred_element_type=jnp.float32)
        pieces = [
            projected[:, idx * slim : (idx + 1) * slim].astype(jnp.bfloat16) for idx in range(6)
        ]
        arrived = (
            lax.all_to_all(as_sent(pieces[0]), "dp", split_axis=0, concat_axis=1, tiled=True),
            lax.all_to_all(as_sent(pieces[1]), "dp", split_axis=0, concat_axis=1, tiled=True),
            lax.all_to_all(as_sent(pieces[2]), "dp", split_axis=0, concat_axis=1, tiled=True),
            lax.all_to_all(as_sent(pieces[3]), "dp", split_axis=0, concat_axis=1, tiled=True),
            lax.all_to_all(as_sent(pieces[4]), "dp", split_axis=0, concat_axis=1, tiled=True),
            lax.all_to_all(as_sent(pieces[5]), "dp", split_axis=0, concat_axis=1, tiled=True),
        )
        recept, key_vec, value_vec, decay_pre, rate_pre, gate_pre = [
            item.astype(jnp.float32) for item in arrived
        ]
        decay_rate = jnp.exp(-jnp.exp(-jax.nn.softplus(-(decay_base[layer_idx] + decay_pre)) - 0.5))
        learn_rate = jax.nn.sigmoid(rate_base[layer_idx] + rate_pre)
        gate_open = jax.nn.sigmoid(gate_pre)
        updated, normal_out = recur(
            state[layer_idx], recept, key_vec, value_vec, decay_rate, learn_rate, active, head_size
        )
        updated_states.append(updated)
        mixed_here = jnp.where(
            active[:, None], normal_out * group_gain[layer_idx] * gate_open, 0.0
        ).astype(jnp.bfloat16)
        rows_all = lax.all_gather(mixed_here, "dp", axis=0, tiled=True)
        out_weight = w_out[layer_idx]

        def fold_output(acc_sum, segment, offset):
            weight_rows = lax.dynamic_slice_in_dim(out_weight, offset, segment.shape[1], 0)
            return acc_sum + jnp.dot(segment, weight_rows, preferred_element_type=jnp.float32)

        blank = jnp.zeros((rows_all.shape[0], out_weight.shape[1]), jnp.float32)
        out_cols = taken_in(rows_all, "tp", 1, fold_output, blank).astype(jnp.bfloat16)
        current = lax.all_to_all(out_cols, "dp", split_axis=0, concat_axis=1, tiled=True)
    return (current, jnp.stack(updated_states))


def solution(mesh):
    in_specs = (
        P("dp", "tp"),
        P("dp"),
        P(),
        P(None, None, ("tp", "dp")),
        P(None, None, ("tp", "dp")),
        P(None, None, ("tp", "dp")),
        P(None, None, ("tp", "dp")),
        P(None, None, ("tp", "dp")),
        P(None, None, ("tp", "dp")),
        P(None, None, ("tp", "dp")),
        P(None, "tp"),
        P(None, "tp"),
        P(None, "tp"),
        P(None, "dp", "tp", None, None),
    )
    out_specs = (P("dp", "tp"), P(None, "dp", "tp", None, None))
    return jax.shard_map(
        on_device, mesh=mesh, in_specs=in_specs, out_specs=out_specs, check_vma=False
    )
```

profile of v0, /device:TPU:0, one launch (start us, length us, event | category | flops | bytes accessed | tf_op | source)
XLA Modules:
  0.0 371.2 jit_solution(15429060833024685349)
XLA Ops:
  7.2 8.5 %all_gather.24 = bf16[128,512]{1,0:T(8,128)(2,1)} all-gather(bf16[32,512]{1,0:T(8,128)(2,1)} %param.14), channel_id=1, replica_groups=mesh['tp'=8,'dp'=4] {'dp'}, dimensions={0}, use_global_device_ids=true | all-gather | bytes 163840 | tf_op jit(solution)/shard_map/all_gather | solution.py:83
  29.2 26.6 %all-gather.5.cloned.1.call-done = bf16[128,4096]{1,0:T(8,128)(2,1)} async-done(((bf16[128,512]{1,0:T(8,128)(2,1)}), bf16[128,4096]{1,0:T(8,128)(2,1)}) %all-gather.5.cloned.1.call-update) | async-done | bytes 1048592 | tf_op jit(solution)/shard_map/all_gather | solution.py:84
  57.4 4.2 %convolution_convert_fusion.1 = bf16[128,768]{1,0:T(8,128)(2,1)S(1)} fusion(bf16[4096,768]{1,0:T(8,128)(2,1)} %get-tuple-element.8, bf16[128,4096]{1,0:T(8,128)(2,1)} %all-gather.5.cloned.1.call-done, f32[4096]{0:T(1024)S(1)} %bitcast.161, f32[128]{0:T(128)S(1)} %add_rsqrt_fusion.3), kind=kOutput, calls=%fused_computation.48 | convolution fusion | flops 807501824 | bytes 7553536 | tf_op jit(solution)/shard_map/dot_general | solution.py:88
  65.5 3.9 %all-to-all-done.4 = bf16[4,32,128]{2,1,0:T(8,128)(2,1)S(1)} async-done(((bf16[4,32,128]{2,1,0:T(8,128)(2,1)}), bf16[4,32,128]{2,1,0:T(8,128)(2,1)S(1)}, u32[]{:S(2)}, u32[]{:S(2)}) %all-to-all-start.4) | async-done | bytes 32800 | tf_op jit(solution)/shard_map/all_to_all | solution.py:93
  72.9 3.7 all-to-all-done.1
  79.9 3.9 %all-to-all-done.2 = bf16[4,32,128]{2,1,0:T(8,128)(2,1)S(1)} async-done(((bf16[4,32,128]{2,1,0:T(8,128)(2,1)}), bf16[4,32,128]{2,1,0:T(8,128)(2,1)S(1)}, u32[]{:S(2)}, u32[]{:S(2)}) %all-to-all-start.2) | async-done | bytes 32800 | tf_op jit(solution)/shard_map/all_to_all | solution.py:97
  87.1 3.9 %all-to-all-done.3 = bf16[4,32,128]{2,1,0:T(8,128)(2,1)S(1)} async-done(((bf16[4,32,128]{2,1,0:T(8,128)(2,1)}), bf16[4,32,128]{2,1,0:T(8,128)(2,1)S(1)}, u32[]{:S(2)}, u32[]{:S(2)}) %all-to-all-start.3) | async-done | bytes 32800 | tf_op jit(solution)/shard_map/all_to_all | solution.py:95
  91.0 3.3 all-to-all-start
  94.4 3.7 all-to-all-done
  98.1 3.3 all-to-all-start.5
  102.4 15.4 %fusion = f32[32,8,1,64]{3,2,1,0:T(1,128)S(1)} fusion(f32[32,8,64,1]{2,3,1,0:T(1,128)S(1)} %bitcast.154, f32[2,32,8,64,64]{4,3,2,1,0:T(8,128)} %param.27), kind=kOutput, calls=%fused_computation.2 | convolution fusion | flops 12582912 | bytes 8519680 | tf_op jit(solution)/shard_map/bhij,bhj->bhi/dot_general | solution.py:36
  117.8 11.1 %fusion.4 = f32[32,8,1,64]{3,2,1,0:T(1,128)S(1)} fusion(bf16[32,8,64,1]{2,3,1,0:T(2,128)(2,1)S(1)} %reshape.317, f32[2,32,8,64,64]{4,3,2,1,0:T(8,128)} %param.27, f32[32,8,64]{2,1,0:T(8,128)S(1)} %get-tuple-element.23, f32[32,8,64]{2,1,0:T(8,128)S(1)} %reshape.299, f32[32,8,64]{2,1,0:T(8,128)S(1)} %get-tuple-element.22, f32[32,8,64]{2,1,0:T(8,128)S(1)} %bitcast.150, ...), kind=kOutput, calls=%fused_computation.7 | convolution fusion | flops 18874368 | bytes 8814624 | tf_op jit(solution)/shard_map/bhij,bhj->bhi/dot_general | solution.py:43
  129.5 6.1 %all_gather.26 = bf16[128,512]{1,0:T(8,128)(2,1)} all-gather(bf16[32,512]{1,0:T(8,128)(2,1)S(1)} %fusion.59), channel_id=1, replica_groups=mesh['tp'=8,'dp'=4] {'dp'}, dimensions={0}, use_global_device_ids=true | all-gather | bytes 163840 | tf_op jit(solution)/shard_map/all_gather | solution.py:113
  135.7 39.3 %all-gather.7.cloned.1.call-done = bf16[128,4096]{1,0:T(8,128)(2,1)} async-done(((bf16[128,512]{1,0:T(8,128)(2,1)}), bf16[128,4096]{1,0:T(8,128)(2,1)}) %all-gather.7.cloned.1.call-update) | async-done | bytes 1048592 | tf_op jit(solution)/shard_map/all_gather | solution.py:22
  177.0 6.5 %all_to_all.200 = bf16[4,32,128]{2,1,0:T(8,128)(2,1)S(1)} all-to-all(bf16[4,32,128]{2,1,0:T(8,128)(2,1)S(1)} %bitcast.159), channel_id=1, replica_groups=mesh['tp'=8,'dp'=4] {'dp'}, dimensions={0} | all-to-all | bytes 65536 | tf_op jit(solution)/shard_map/all_to_all | solution.py:122
  183.5 5.9 %all_gather.28 = bf16[128,512]{1,0:T(8,128)(2,1)} all-gather(bf16[32,512]{1,0:T(8,128)(2,1)S(1)} %copy_bitcast_fusion.1), channel_id=1, replica_groups=mesh['tp'=8,'dp'=4] {'dp'}, dimensions={0}, use_global_device_ids=true | all-gather | bytes 163840 | tf_op jit(solution)/shard_map/all_gather | solution.py:83
  189.3 38.1 %all-gather.9.cloned.1.call-done = bf16[128,4096]{1,0:T(8,128)(2,1)} async-done(((bf16[128,512]{1,0:T(8,128)(2,1)}), bf16[128,4096]{1,0:T(8,128)(2,1)}) %all-gather.9.cloned.1.call-update) | async-done | bytes 1048592 | tf_op jit(solution)/shard_map/all_gather | solution.py:84
  228.9 4.2 %convolution_convert_fusion = bf16[128,768]{1,0:T(8,128)(2,1)S(1)} fusion(bf16[4096,768]{1,0:T(8,128)(2,1)} %get-tuple-element.9, bf16[128,4096]{1,0:T(8,128)(2,1)} %all-gather.9.cloned.1.call-done, f32[4096]{0:T(1024)S(1)} %bitcast.160, f32[128]{0:T(128)S(1)} %add_rsqrt_fusion.2), kind=kOutput, calls=%fused_computation.47 | convolution fusion | flops 807501824 | bytes 7553536 | tf_op jit(solution)/shard_map/dot_general | solution.py:88
  233.8 6.5 %all_to_all.201 = bf16[4,32,128]{2,1,0:T(8,128)(2,1)S(1)} all-to-all(bf16[4,32,128]{2,1,0:T(8,128)(2,1)S(1)} %bitcast.156), channel_id=1, replica_groups=mesh['tp'=8,'dp'=4] {'dp'}, dimensions={0} | all-to-all | bytes 65536 | tf_op jit(solution)/shard_map/all_to_all | solution.py:93
  243.7 3.8 %all-to-all-done.8 = bf16[4,32,128]{2,1,0:T(8,128)(2,1)S(1)} async-done(((bf16[4,32,128]{2,1,0:T(8,128)(2,1)}), bf16[4,32,128]{2,1,0:T(8,128)(2,1)S(1)}, u32[]{:S(2)}, u32[]{:S(2)}) %all-to-all-start.8) | async-done | bytes 32800 | tf_op jit(solution)/shard_map/all_to_all | solution.py:94
  250.7 3.9 %all-to-all-done.9 = bf16[4,32,128]{2,1,0:T(8,128)(2,1)S(1)} async-done(((bf16[4,32,128]{2,1,0:T(8,128)(2,1)}), bf16[4,32,128]{2,1,0:T(8,128)(2,1)S(1)}, u32[]{:S(2)}, u32[]{:S(2)}) %all-to-all-start.9) | async-done | bytes 32800 | tf_op jit(solution)/shard_map/all_to_all | solution.py:97
  257.9 3.9 %all-to-all-done.10 = bf16[4,32,128]{2,1,0:T(8,128)(2,1)S(1)} async-done(((bf16[4,32,128]{2,1,0:T(8,128)(2,1)}), bf16[4,32,128]{2,1,0:T(8,128)(2,1)S(1)}, u32[]{:S(2)}, u32[]{:S(2)}) %all-to-all-start.10) | async-done | bytes 32800 | tf_op jit(solution)/shard_map/all_to_all | solution.py:95
  261.8 3.3 all-to-all-start.7
  265.3 3.7 all-to-all-done.7
  269.0 3.3 all-to-all-start.12
  273.1 15.4 %fusion.5 = f32[32,8,1,64]{3,2,1,0:T(1,128)S(1)} fusion(f32[32,8,64,1]{2,3,1,0:T(1,128)S(1)} %bitcast.155, f32[2,32,8,64,64]{4,3,2,1,0:T(8,128)} %param.27), kind=kOutput, calls=%fused_computation.9 | convolution fusion | flops 12582912 | bytes 8519680 | tf_op jit(solution)/shard_map/bhij,bhj->bhi/dot_general | solution.py:36
  288.6 11.1 %fusion.9 = f32[32,8,1,64]{3,2,1,0:T(1,128)S(1)} fusion(bf16[32,8,64,1]{2,3,1,0:T(2,128)(2,1)S(1)} %reshape.319, f32[2,32,8,64,64]{4,3,2,1,0:T(8,128)} %param.27, f32[32,8,64]{2,1,0:T(8,128)S(1)} %get-tuple-element.21, f32[32,8,64]{2,1,0:T(8,128)S(1)} %reshape.305, f32[32,8,64]{2,1,0:T(8,128)S(1)} %get-tuple-element.20, f32[32,8,64]{2,1,0:T(8,128)S(1)} %bitcast.152, ...), kind=kOutput, calls=%fused_computation.14 | convolution fusion | flops 18874368 | bytes 8814624 | tf_op jit(solution)/shard_map/bhij,bhj->bhi/dot_general | solution.py:43
  300.3 5.9 %all_gather.30 = bf16[128,512]{1,0:T(8,128)(2,1)} all-gather(bf16[32,512]{1,0:T(8,128)(2,1)S(1)} %fusion.57), channel_id=1, replica_groups=mesh['tp'=8,'dp'=4] {'dp'}, dimensions={0}, use_global_device_ids=true | all-gather | bytes 163840 | tf_op jit(solution)/shard_map/all_gather | solution.py:113
  306.3 13.7 %add_select_fusion.1 = (f32[1,32,8,64,64]{4,3,2,1,0:T(8,128)}, f32[1,32,8,64,64]{4,3,2,1,0:T(8,128)}) fusion(f32[2,32,8,64,64]{4,3,2,1,0:T(8,128)} %param.27, f32[32,8,64]{2,1,0:T(8,128)S(1)} %get-tuple-element.23, f32[32,8,64]{2,1,0:T(8,128)S(1)} %reshape.299, f32[32,8,64]{2,1,0:T(8,128)S(1)} %get-tuple-element.22, f32[32,8,64]{2,1,0:T(8,128)S(1)} %bitcast.151, ...), kind=kLoop, calls=%fused_computation.16 | loop fusion | flops 12582912 | bytes 17432608 | tf_op jit(solution)/shard_map/jit(_where)/select_n | solution.py:42
  320.0 25.7 %all-gather.11.cloned.1.call-done = bf16[128,4096]{1,0:T(8,128)(2,1)} async-done(((bf16[128,512]{1,0:T(8,128)(2,1)}), bf16[128,4096]{1,0:T(8,128)(2,1)}) %all-gather.11.cloned.1.call-update) | async-done | bytes 1048592 | tf_op jit(solution)/shard_map/all_gather | solution.py:22
  348.3 3.3 all-to-all-start.13
  351.5 12.5 %pad_maximum_fusion = f32[2,32,8,64,64]{4,3,2,1,0:T(8,128)} fusion(f32[1,32,8,64,64]{4,3,2,1,0:T(8,128)} %get-tuple-element.7, f32[1,32,8,64,64]{4,3,2,1,0:T(8,128)} %get-tuple-element.6), kind=kLoop, calls=%fused_computation | loop fusion | flops 2097152 | bytes 16777216 | tf_op jit(solution)/shard_map/stack | solution.py:123
  (108 shorter events, 49.8 us)
Async XLA Ops:
  7.2 15.8 %copy-start = (bf16[2,4096,128]{2,1,0:T(8,128)(2,1)S(1)}, bf16[2,4096,128]{2,1,0:T(8,128)(2,1)}, u32[]{:S(2)}) copy-start(bf16[2,4096,128]{2,1,0:T(8,128)(2,1)} %param.19) | copy-start | bytes 6291460
  7.2 48.7 %all-gather.5.cloned.1.call-start = ((), (), s32[]{:S(2)}) async-start(), calls=%async_computation.14 | async-start | bytes 1179648 | tf_op jit(solution)/shard_map/all_gather | solution.py:84
  16.6 8.0 %copy-start.1 = (bf16[2,4096,128]{2,1,0:T(8,128)(2,1)S(1)}, bf16[2,4096,128]{2,1,0:T(8,128)(2,1)}, u32[]{:S(2)}) copy-start(bf16[2,4096,128]{2,1,0:T(8,128)(2,1)} %param.20) | copy-start | bytes 6291460
  19.8 6.3 %copy-start.2 = (bf16[2,4096,128]{2,1,0:T(8,128)(2,1)S(1)}, bf16[2,4096,128]{2,1,0:T(8,128)(2,1)}, u32[]{:S(2)}) copy-start(bf16[2,4096,128]{2,1,0:T(8,128)(2,1)} %param.21) | copy-start | bytes 6291460
  23.0 4.6 %copy-start.4 = (f32[2,4096]{1,0:T(2,128)S(1)}, f32[2,4096]{1,0:T(2,128)}, u32[]{:S(2)}) copy-start(f32[2,4096]{1,0:T(2,128)} %param.16) | copy-start | bytes 98308
  23.0 4.6 %copy-start.3 = (bf16[2,4096,128]{2,1,0:T(8,128)(2,1)S(1)}, bf16[2,4096,128]{2,1,0:T(8,128)(2,1)}, u32[]{:S(2)}) copy-start(bf16[2,4096,128]{2,1,0:T(8,128)(2,1)} %param.22) | copy-start | bytes 6291460
  27.6 37.9 %copy-start.7 = (s32[32]{0:T(128)S(1)}, s32[32]{0:T(128)}, u32[]{:S(2)}) copy-start(s32[32]{0:T(128)} %param.15) | copy-start | bytes 388
  27.7 45.0 %copy-start.5 = (f32[2,512]{1,0:T(2,128)S(1)}, f32[2,512]{1,0:T(2,128)}, u32[]{:S(2)}) copy-start(f32[2,512]{1,0:T(2,128)} %param.25) | copy-start | bytes 12292
  27.7 45.0 %copy-start.6 = (f32[2,512]{1,0:T(2,128)S(1)}, f32[2,512]{1,0:T(2,128)}, u32[]{:S(2)}) copy-start(f32[2,512]{1,0:T(2,128)} %param.24) | copy-start | bytes 12292
  62.2 7.2 %all-to-all-start.4 = ((bf16[4,32,128]{2,1,0:T(8,128)(2,1)}), bf16[4,32,128]{2,1,0:T(8,128)(2,1)S(1)}, u32[]{:S(2)}, u32[]{:S(2)}) async-start(bf16[4,32,128]{2,1,0:T(8,128)(2,1)} %bitcast.21), calls=%async_computation.4 | async-start | bytes 65536 | tf_op jit(solution)/shard_map/all_to_all | solution.py:93
  69.4 7.2 %all-to-all-start.1 = ((bf16[4,32,128]{2,1,0:T(8,128)(2,1)}), bf16[4,32,128]{2,1,0:T(8,128)(2,1)S(1)}, u32[]{:S(2)}, u32[]{:S(2)}) async-start(bf16[4,32,128]{2,1,0:T(8,128)(2,1)} %bitcast.11), calls=%async_computation.1 | async-start | bytes 65536 | tf_op jit(solution)/shard_map/all_to_all | solution.py:94
  76.6 7.2 %all-to-all-start.2 = ((bf16[4,32,128]{2,1,0:T(8,128)(2,1)}), bf16[4,32,128]{2,1,0:T(8,128)(2,1)S(1)}, u32[]{:S(2)}, u32[]{:S(2)}) async-start(bf16[4,32,128]{2,1,0:T(8,128)(2,1)} %bitcast.17), calls=%async_computation.2 | async-start | bytes 65536 | tf_op jit(solution)/shard_map/all_to_all | solution.py:97
  83.8 7.2 %all-to-all-start.3 = ((bf16[4,32,128]{2,1,0:T(8,128)(2,1)}), bf16[4,32,128]{2,1,0:T(8,128)(2,1)S(1)}, u32[]{:S(2)}, u32[]{:S(2)}) async-start(bf16[4,32,128]{2,1,0:T(8,128)(2,1)} %bitcast.19), calls=%async_computation.3 | async-start | bytes 65536 | tf_op jit(solution)/shard_map/all_to_all | solution.py:95
  91.0 7.2 %all-to-all-start = ((bf16[4,32,128]{2,1,0:T(8,128)(2,1)}), bf16[4,32,128]{2,1,0:T(8,128)(2,1)S(1)}, u32[]{:S(2)}, u32[]{:S(2)}) async-start(bf16[4,32,128]{2,1,0:T(8,128)(2,1)} %bitcast.9), calls=%async_computation | async-start | bytes 65536 | tf_op jit(solution)/shard_map/all_to_all | solution.py:96
  98.1 31.3 %all-to-all-start.5 = ((bf16[4,32,128]{2,1,0:T(8,128)(2,1)}), bf16[4,32,128]{2,1,0:T(8,128)(2,1)S(1)}, u32[]{:S(2)}, u32[]{:S(2)}) async-start(bf16[4,32,128]{2,1,0:T(8,128)(2,1)} %bitcast.26), calls=%async_computation.5 | async-start | bytes 65536 | tf_op jit(solution)/shard_map/all_to_all | solution.py:98
  101.4 73.6 %all-gather.7.cloned.1.call-start = ((), (), s32[]{:S(2)}) async-start(), calls=%async_computation.15 | async-start | bytes 1179648 | tf_op jit(solution)/shard_map/all_gather | solution.py:22
  135.6 91.8 %all-gather.9.cloned.1.call-start = ((), (), s32[]{:S(2)}) async-start(), calls=%async_computation.16 | async-start | bytes 1179648 | tf_op jit(solution)/shard_map/all_gather | solution.py:84
  240.2 7.2 %all-to-all-start.8 = ((bf16[4,32,128]{2,1,0:T(8,128)(2,1)}), bf16[4,32,128]{2,1,0:T(8,128)(2,1)S(1)}, u32[]{:S(2)}, u32[]{:S(2)}) async-start(bf16[4,32,128]{2,1,0:T(8,128)(2,1)} %bitcast.40), calls=%async_computation.8 | async-start | bytes 65536 | tf_op jit(solution)/shard_map/all_to_all | solution.py:94
  247.4 7.2 %all-to-all-start.9 = ((bf16[4,32,128]{2,1,0:T(8,128)(2,1)}), bf16[4,32,128]{2,1,0:T(8,128)(2,1)S(1)}, u32[]{:S(2)}, u32[]{:S(2)}) async-start(bf16[4,32,128]{2,1,0:T(8,128)(2,1)} %bitcast.46), calls=%async_computation.9 | async-start | bytes 65536 | tf_op jit(solution)/shard_map/all_to_all | solution.py:97
  254.6 7.2 %all-to-all-start.10 = ((bf16[4,32,128]{2,1,0:T(8,128)(2,1)}), bf16[4,32,128]{2,1,0:T(8,128)(2,1)S(1)}, u32[]{:S(2)}, u32[]{:S(2)}) async-start(bf16[4,32,128]{2,1,0:T(8,128)(2,1)} %bitcast.48), calls=%async_computation.10 | async-start | bytes 65536 | tf_op jit(solution)/shard_map/all_to_all | solution.py:95
  261.8 7.2 %all-to-all-start.7 = ((bf16[4,32,128]{2,1,0:T(8,128)(2,1)}), bf16[4,32,128]{2,1,0:T(8,128)(2,1)S(1)}, u32[]{:S(2)}, u32[]{:S(2)}) async-start(bf16[4,32,128]{2,1,0:T(8,128)(2,1)} %bitcast.38), calls=%async_computation.7 | async-start | bytes 65536 | tf_op jit(solution)/shard_map/all_to_all | solution.py:96
  269.0 31.3 %all-to-all-start.12 = ((bf16[4,32,128]{2,1,0:T(8,128)(2,1)}), bf16[4,32,128]{2,1,0:T(8,128)(2,1)S(1)}, u32[]{:S(2)}, u32[]{:S(2)}) async-start(bf16[4,32,128]{2,1,0:T(8,128)(2,1)} %bitcast.55), calls=%async_computation.12 | async-start | bytes 65536 | tf_op jit(solution)/shard_map/all_to_all | solution.py:98
  272.2 73.4 %all-gather.11.cloned.1.call-start = ((), (), s32[]{:S(2)}) async-start(), calls=%async_computation.17 | async-start | bytes 1179648 | tf_op jit(solution)/shard_map/all_gather | solution.py:22
  348.3 15.8 %all-to-all-start.13 = ((bf16[4,32,128]{2,1,0:T(8,128)(2,1)}), bf16[4,32,128]{2,1,0:T(8,128)(2,1)S(1)}, u32[]{:S(2)}, u32[]{:S(2)}) async-start(bf16[4,32,128]{2,1,0:T(8,128)(2,1)} %bitcast.58), calls=%async_computation.13 | async-start | bytes 65536 | tf_op jit(solution)/shard_map/all_to_all | solution.py:122
Sparse Core Ops, SparseCore 0:
  15.9 39.8 all-gather.4
  135.8 39.2 all-gather.6
  189.5 37.9 all-gather.8
  306.4 39.2 all-gather.10
where the time goes:
time: 373 us; the launch traced here: 371 us
  waiting for transfers between devices  164 us (44%)
  matrix products  65.8 us (18%)
  starting transfers between devices  39.3 us (11%)
  blocking collectives  39.3 us (11%)
  other arithmetic  31 us (8%)
  local copies, waits for them, and re-layouts  17.3 us (5%)
  between operations  14.3 us (4%)
    all_gather x2, waiting for transfers between devices, gathered(): return lax.all_gather(part, axis, axis=dim, tiled=True)  65.1 us
    all_gather x2, waiting for transfers between devices, on_device(): every_feature = lax.all_gather(batch_raw, 'tp', axis=1, tiled=True)  64.7 us
    dot_general x2, matrix products, recur(): jnp.einsum('bhij,bhj->bhi', state_old, -key_unit, precision=lax.Precision...  30.8 us
    dot_general x2, matrix products, recur(): jnp.einsum('bhij,bhj->bhi', updated, recept_h, precision=lax.Precision.HI...  22.1 us
    all_gather x2, blocking collectives, on_device(): batch_raw = lax.all_gather(current, 'dp', axis=0, tiled=True)  14.4 us
    select_n x1, other arithmetic, recur(): updated = jnp.where(active[:, None, None, None], updated, state_old)  13.7 us
    another operation x1, other arithmetic, on_device(): return (current, jnp.stack(updated_states))  12.5 us
    all_gather x2, blocking collectives, on_device(): rows_all = lax.all_gather(mixed_here, 'dp', axis=0, tiled=True)  12 us
  transfers between devices with their start and end apart: 16, of which 13 were waited for; matrix products, arithmetic and copies ran while one was open for 26% of the time, Pallas kernels for 0%

commit v1 on v0

v1 whole, which is shorter than its diff:
```python
import functools

import jax
import jax.numpy as jnp
from jax import lax
from jax.experimental import pallas as pl
from jax.experimental.pallas import tpu as pltpu
from jax.sharding import PartitionSpec as P

STEP = 16
RMS_EPS = 1e-06
GROUP_EPS = 0.00064
VMEM_LIMIT = 56 * 1024 * 1024


def project_body(x_ref, gain_ref, *refs, features, steps):
    weights, out_ref, acc, square = refs[:6], refs[6], refs[7], refs[8]
    step = pl.program_id(0)
    slim = weights[0].shape[-1]

    @pl.when(step == 0)
    def _():
        acc[...] = jnp.zeros_like(acc)
        square[...] = jnp.zeros_like(square)

    values = x_ref[...].astype(jnp.float32)
    square[...] += jnp.sum(values * values, axis=1, keepdims=True)
    scaled = (values * gain_ref[...]).astype(jnp.bfloat16)
    if slim % 128 == 0:
        joined = jnp.concatenate([w[0] for w in weights], axis=1)
        total = jnp.dot(scaled, joined, preferred_element_type=jnp.float32)
        for idx in range(6):
            acc[idx] += total[:, idx * slim : (idx + 1) * slim]
    else:
        for idx in range(6):
            acc[idx] += jnp.dot(scaled, weights[idx][0], preferred_element_type=jnp.float32)

    @pl.when(step == steps - 1)
    def _():
        factor = lax.rsqrt(square[...] / features + RMS_EPS)
        for idx in range(6):
            out_ref[idx] = (acc[idx] * factor).astype(out_ref.dtype)


def project(x, gain, weights, layer):
    rows, features = x.shape
    slim = weights[0].shape[2]
    depth = 512
    steps = features // depth
    return pl.pallas_call(
        functools.partial(project_body, features=features, steps=steps),
        grid=(steps,),
        out_shape=jax.ShapeDtypeStruct((6, rows, slim), jnp.bfloat16),
        in_specs=[
            pl.BlockSpec((rows, depth), lambda i: (0, i)),
            pl.BlockSpec((1, depth), lambda i: (0, i)),
        ]
        + [pl.BlockSpec((1, depth, slim), lambda i: (layer, i, 0))] * 6,
        out_specs=pl.BlockSpec((6, rows, slim), lambda i: (0, 0, 0)),
        scratch_shapes=[
            pltpu.VMEM((6, rows, slim), jnp.float32),
            pltpu.VMEM((rows, 1), jnp.float32),
        ],
        compiler_params=pltpu.CompilerParams(vmem_limit_bytes=VMEM_LIMIT),
        name="project",
    )(x, gain, *weights)


def fold_body(x_ref, w_ref, out_ref, acc, *, steps):
    step = pl.program_id(0)

    @pl.when(step == 0)
    def _():
        acc[...] = jnp.zeros_like(acc)

    acc[...] += jnp.dot(x_ref[...], w_ref[0], preferred_element_type=jnp.float32)

    @pl.when(step == steps - 1)
    def _():
        out_ref[...] = acc[...].astype(out_ref.dtype)


def fold(x, weight, layer):
    rows, features = x.shape
    slim = weight.shape[2]
    depth = 1024
    steps = features // depth
    return pl.pallas_call(
        functools.partial(fold_body, steps=steps),
        grid=(steps,),
        out_shape=jax.ShapeDtypeStruct((rows, slim), jnp.bfloat16),
        in_specs=[
            pl.BlockSpec((rows, depth), lambda i: (0, i)),
            pl.BlockSpec((1, depth, slim), lambda i: (layer, i, 0)),
        ],
        out_specs=pl.BlockSpec((rows, slim), lambda i: (0, 0)),
        scratch_shapes=[pltpu.VMEM((rows, slim), jnp.float32)],
        compiler_params=pltpu.CompilerParams(vmem_limit_bytes=VMEM_LIMIT),
        name="fold",
    )(x, weight)


def recur_body(vec_ref, lens_ref, base_ref, rate_ref, gain_ref, state_ref, *refs):
    new_ref, mixed_ref, rows_s, read_s = refs[-4:]
    group, heads, size = state_ref.shape[1], state_ref.shape[2], state_ref.shape[3]
    live = lens_ref[...] > STEP
    for h in range(heads):
        part = slice(h * size, (h + 1) * size)
        recept, key, value, decay_pre, rate_pre = [
            vec_ref[q, :, part].astype(jnp.float32) for q in range(5)
        ]
        decay = jnp.exp(-jnp.exp(-jax.nn.softplus(-(base_ref[:, part] + decay_pre)) - 0.5))
        rate = jax.nn.sigmoid(rate_ref[:, part] + rate_pre)
        length = jnp.maximum(jnp.sqrt(jnp.sum(key * key, axis=1, keepdims=True)), 1e-12)
        unit = key / length
        rows_s[0, h] = -unit
        rows_s[1, h] = value * length
        rows_s[2, h] = decay
        rows_s[3, h] = unit * rate
        rows_s[4, h] = recept
    across = lax.broadcasted_iota(jnp.int32, (size, size), 0)
    along = lax.broadcasted_iota(jnp.int32, (size, size), 1)
    eye = across == along

    def one(b, carry):
        keep = lens_ref[pl.ds(b, 1), :size] > STEP
        for h in range(heads):
            neg, held, decay, rated, recept = [rows_s[q, h, pl.ds(b, 1), :] for q in range(5)]
            old = state_ref[0, b, h]
            terms = old * neg + jnp.where(eye, held, 0.0)
            weight = jnp.sum(terms, axis=1, keepdims=True)
            updated = old * decay + weight * rated
            new_ref[0, b, h] = jnp.where(keep, updated, old)
            read = jnp.sum(updated * recept, axis=1, keepdims=True)
            read_s[h, pl.ds(b, 1), :] = jnp.sum(jnp.where(eye, read, 0.0), axis=0, keepdims=True)
        return carry

    lax.fori_loop(0, group, one, 0)
    for h in range(heads):
        part = slice(h * size, (h + 1) * size)
        read = read_s[h]
        centre = jnp.mean(read, axis=1, keepdims=True)
        apart = read - centre
        spread = jnp.mean(apart * apart, axis=1, keepdims=True)
        normal = apart * lax.rsqrt(spread + GROUP_EPS) * gain_ref[:, part]
        gate = jax.nn.sigmoid(vec_ref[5, :, part].astype(jnp.float32))
        mixed_ref[:, part] = jnp.where(live[:, :size], normal * gate, 0.0).astype(mixed_ref.dtype)


def recur(vec, lens, base, rate, gain, state, earlier, layer):
    _, rows, width = vec.shape
    heads, size = state.shape[2], state.shape[3]
    group = 8
    block = pl.BlockSpec((1, group, heads, size, size), lambda i: (layer, i, 0, 0, 0))
    line = pl.BlockSpec((1, width), lambda i: (0, 0))
    operands = [vec, lens, base, rate, gain, state]
    in_specs = [
        pl.BlockSpec((6, group, width), lambda i: (0, i, 0)),
        pl.BlockSpec((group, lens.shape[1]), lambda i: (i, 0)),
        line,
        line,
        line,
        block,
    ]
    aliases = {}
    if earlier is not None:
        operands.append(earlier)
        in_specs.append(pl.BlockSpec(memory_space=pl.ANY))
        aliases = {6: 0}
    return pl.pallas_call(
        recur_body,
        grid=(rows // group,),
        out_shape=(
            jax.ShapeDtypeStruct(state.shape, state.dtype),
            jax.ShapeDtypeStruct((rows, width), jnp.bfloat16),
        ),
        in_specs=in_specs,
        out_specs=(block, pl.BlockSpec((group, width), lambda i: (i, 0))),
        scratch_shapes=[
            pltpu.VMEM((5, heads, group, size), jnp.float32),
            pltpu.VMEM((heads, group, size), jnp.float32),
        ],
        input_output_aliases=aliases,
        compiler_params=pltpu.CompilerParams(vmem_limit_bytes=VMEM_LIMIT),
        name="recur",
    )(*operands)


def on_device(
    tokens,
    lengths,
    norm_gain,
    w_recept,
    w_key,
    w_value,
    w_decay,
    w_rate,
    w_gate,
    w_out,
    decay_base,
    rate_base,
    group_gain,
    state,
):
    weights = (w_recept, w_key, w_value, w_decay, w_rate, w_gate)
    lens = jnp.broadcast_to(lengths[:, None], (lengths.shape[0], 128))
    every = lax.all_gather(tokens, "dp", axis=0, tiled=True)
    every = lax.all_gather(every, "tp", axis=1, tiled=True)
    states = None
    for layer in range(2):
        pick = slice(layer, layer + 1)
        pieces = project(every, norm_gain[pick], weights, layer)
        vec = lax.all_to_all(pieces, "dp", split_axis=1, concat_axis=2, tiled=True)
        states, mixed = recur(
            vec, lens, decay_base[pick], rate_base[pick], group_gain[pick], state, states, layer
        )
        rows_all = lax.all_gather(mixed, "dp", axis=0, tiled=True)
        rows_all = lax.all_gather(rows_all, "tp", axis=1, tiled=True)
        columns = fold(rows_all, w_out, layer)
        if layer == 0:
            every = lax.all_gather(columns, ("tp", "dp"), axis=1, tiled=True)
    current = lax.all_to_all(columns, "dp", split_axis=0, concat_axis=1, tiled=True)
    return (current, states)


def solution(mesh):
    in_specs = (
        P("dp", "tp"),
        P("dp"),
        P(),
        P(None, None, ("tp", "dp")),
        P(None, None, ("tp", "dp")),
        P(None, None, ("tp", "dp")),
        P(None, None, ("tp", "dp")),
        P(None, None, ("tp", "dp")),
        P(None, None, ("tp", "dp")),
        P(None, None, ("tp", "dp")),
        P(None, "tp"),
        P(None, "tp"),
        P(None, "tp"),
        P(None, "dp", "tp", None, None),
    )
    out_specs = (P("dp", "tp"), P(None, "dp", "tp", None, None))
    return jax.shard_map(
        on_device, mesh=mesh, in_specs=in_specs, out_specs=out_specs, check_vma=False
    )
```

time: 373 us -> 283 us (0.76)
  matrix products: 65.8 us -> 0 us
  Pallas kernels: 0 us -> 46.3 us
  starting transfers between devices: 39.3 us -> 3.57 us
  other arithmetic: 31 us -> 0 us
  waiting for transfers between devices: 164 us -> 172 us
  local copies, waits for them, and re-layouts: 17.3 us -> 9.36 us
    dot_general x8 -> x0, matrix products: 65.8 us -> none  [the longest x2 30.8 us: recur(): jnp.einsum('bhij,bhj->bhi', state_old, -key_unit, precision=lax.Precision...]
    pallas_call x0 -> x6, Pallas kernels: none -> 46.3 us  [the longest x2 24.9 us: recur(): pl.pallas_call(recur_body, grid=(rows // group,), out_shape=(jax.ShapeDty...]
    all_gather x4, waiting for transfers between devices: 130 us -> 167 us  [the longest x2 78.1 us: on_device(): rows_all = lax.all_gather(rows_all, 'tp', axis=1, tiled=True)]
    all_to_all x12 -> x1, starting transfers between devices: 39.2 us -> 3.41 us  [on_device(): vec = lax.all_to_all(pieces, 'dp', split_axis=1, concat_axis=2, tiled=True)]
    all_to_all x12 -> x1, waiting for transfers between devices: 34.4 us -> 5.31 us  [on_device(): vec = lax.all_to_all(pieces, 'dp', split_axis=1, concat_axis=2, tiled=True)]
    select_n x1 -> x0, other arithmetic: 13.7 us -> none  [recur(): updated = jnp.where(active[:, None, None, None], updated, state_old)]
    another operation x1 -> x0, other arithmetic: 12.5 us -> none  [on_device(): return (current, jnp.stack(updated_states))]
    unnamed x21 -> x4, local copies, waits for them, and re-layouts: 11.1 us -> 0.01 us
  transfers between devices with their start and end apart: 16 -> 5, of which waited for: 13 -> 5; matrix products, arithmetic and copies ran while one was open for 26% -> 1% of each run, Pallas kernels for 0% -> 0%
where the time goes in v1:
time: 283 us; the launch traced here: 282 us
  waiting for transfers between devices  172 us (61%)
  Pallas kernels  46.3 us (16%)
  blocking collectives  36.7 us (13%)
  between operations  13.8 us (5%)
  local copies, waits for them, and re-layouts  9.36 us (3%)
  starting transfers between devices  3.57 us (1%)
    all_gather x2, waiting for transfers between devices, on_device(): rows_all = lax.all_gather(rows_all, 'tp', axis=1, tiled=True)  78.1 us
    all_gather x1, waiting for transfers between devices, on_device(): every = lax.all_gather(columns, ('tp', 'dp'), axis=1, tiled=True)  51.5 us
    all_gather x1, waiting for transfers between devices, on_device(): every = lax.all_gather(every, 'tp', axis=1, tiled=True)  37.2 us
    pallas_call x2, Pallas kernels, recur(): pl.pallas_call(recur_body, grid=(rows // group,), out_shape=(jax.ShapeDty...  24.9 us
    pallas_call x2, Pallas kernels, project(): pl.pallas_call(functools.partial(project_body, features=features, steps=s...  14.6 us
    all_gather x2, blocking collectives, on_device(): rows_all = lax.all_gather(mixed, 'dp', axis=0, tiled=True)  12.1 us
    all_to_all x1, blocking collectives, on_device(): vec = lax.all_to_all(pieces, 'dp', split_axis=1, concat_axis=2, tiled=True)  9.01 us
    all_gather x1, blocking collectives, on_device(): every = lax.all_gather(tokens, 'dp', axis=0, tiled=True)  8.42 us
  transfers between devices with their start and end apart: 5, of which 5 were waited for; matrix products, arithmetic and copies ran while one was open for 1% of the time, Pallas kernels for 0%

profile of v1, /device:TPU:0, one launch (start us, length us, event | category | flops | bytes accessed | tf_op | source)
XLA Modules:
  0.0 281.9 jit_solution(12897289600799569407)
XLA Ops:
  7.2 0.0 all-gather.5.cloned.1.call-start
  7.2 8.4 %all_gather.21 = bf16[128,512]{1,0:T(8,128)(2,1)} all-gather(bf16[32,512]{1,0:T(8,128)(2,1)} %param.14), channel_id=1, replica_groups=mesh['tp'=8,'dp'=4] {'dp'}, dimensions={0}, use_global_device_ids=true | all-gather | bytes 163840 | tf_op jit(solution)/shard_map/all_gather | solution.py:207
  15.6 1.4 fusion.1
  17.0 1.5 fusion
  18.5 37.2 %all-gather.5.cloned.1.call-done.x_ref = bf16[128,4096]{1,0:T(8,128)(2,1)} async-done(((bf16[128,512]{1,0:T(8,128)(2,1)}), bf16[128,4096]{1,0:T(8,128)(2,1)}) %all-gather.5.cloned.1.call-update) | async-done | bytes 1048592 | tf_op jit(solution)/shard_map/all_gather | solution.py:208
  55.7 7.3 %project.2 = bf16[6,128,128]{2,1,0:T(8,128)(2,1)} custom-call(bf16[128,4096]{1,0:T(8,128)(2,1)} %all-gather.5.cloned.1.call-done.x_ref, f32[1,4096]{1,0:T(1,128)} %get-tuple-element.11.gain_ref, bf16[2,4096,128]{2,1,0:T(8,128)(2,1)} %refs_0_.3, bf16[2,4096,128]{2,1,0:T(8,128)(2,1)} %refs_1_.3, bf16[2,4096,128]{2,1,0:T(8,128)(2,1)} %refs_2_.3, ...), custom_call_target="tpu_custom_call" | custom-call | tf_op jit(solution)/shard_map/project/pallas_call | solution.py:50
  63.0 1.8 copy.20
  64.8 3.4 %all-to-all-start = ((bf16[6,128,128]{2,0,1:T(8,128)(2,1)}), bf16[6,128,128]{2,0,1:T(8,128)(2,1)S(1)}, u32[]{:S(2)}, u32[]{:S(2)}) async-start(bf16[6,128,128]{2,0,1:T(8,128)(2,1)} %copy.20), calls=%async_computation | async-start | bytes 524288 | tf_op jit(solution)/shard_map/all_to_all | solution.py:213
  68.2 0.0 all-gather.7.cloned.1.call-start
  68.3 0.6 fusion.3
  68.9 5.3 %all-to-all-done = bf16[6,128,128]{2,0,1:T(8,128)(2,1)S(1)} async-done(((bf16[6,128,128]{2,0,1:T(8,128)(2,1)}), bf16[6,128,128]{2,0,1:T(8,128)(2,1)S(1)}, u32[]{:S(2)}, u32[]{:S(2)}) %all-to-all-start) | async-done | bytes 196640 | tf_op jit(solution)/shard_map/all_to_all | solution.py:213
  74.2 0.2 copy.30
  74.4 0.7 all_to_all.43.vec_ref
  75.1 0.7 broadcast_in_dim.2.lens_ref
  75.8 12.4 %recur.2 = (f32[2,32,8,64,64]{4,3,2,1,0:T(8,128)}, bf16[32,512]{1,0:T(8,128)(2,1)}) custom-call(bf16[6,32,512]{2,1,0:T(8,128)(2,1)} %all_to_all.43.vec_ref, s32[32,128]{1,0:T(8,128)} %broadcast_in_dim.2.lens_ref, f32[1,512]{1,0:T(1,128)} %get-tuple-element.17.base_ref, f32[1,512]{1,0:T(1,128)} %get-tuple-element.18.rate_ref, ...), custom_call_target="tpu_custom_call" | custom-call | tf_op jit(solution)/shard_map/recur/pallas_call | solution.py:170
  88.2 6.1 %all_gather.23 = bf16[128,512]{1,0:T(8,128)(2,1)} all-gather(bf16[32,512]{1,0:T(8,128)(2,1)} %get-tuple-element.6), channel_id=1, replica_groups=mesh['tp'=8,'dp'=4] {'dp'}, dimensions={0}, use_global_device_ids=true | all-gather | bytes 163840 | tf_op jit(solution)/shard_map/all_gather | solution.py:217
  94.3 0.0 all-gather.9.cloned.1.call-start
  94.4 38.8 %all-gather.7.cloned.1.call-done.x_ref = bf16[128,4096]{1,0:T(8,128)(2,1)} async-done(((bf16[128,512]{1,0:T(8,128)(2,1)}), bf16[128,4096]{1,0:T(8,128)(2,1)}) %all-gather.7.cloned.1.call-update) | async-done | bytes 1048592 | tf_op jit(solution)/shard_map/all_gather | solution.py:218
  133.2 3.4 %fold.2 = bf16[128,128]{1,0:T(8,128)(2,1)} custom-call(bf16[128,4096]{1,0:T(8,128)(2,1)} %all-gather.7.cloned.1.call-done.x_ref, bf16[2,4096,128]{2,1,0:T(8,128)(2,1)} %w_ref.3), custom_call_target="tpu_custom_call" | custom-call | tf_op jit(solution)/shard_map/fold/pallas_call | solution.py:88
  136.6 0.0 all-gather.11.cloned.1.call-start
  136.7 51.5 %all-gather.9.cloned.1.call-done.x_ref = bf16[128,4096]{1,0:T(8,128)(2,1)} async-done(((bf16[128,128]{1,0:T(8,128)(2,1)}), bf16[128,4096]{1,0:T(8,128)(2,1)}) %all-gather.9.cloned.1.call-update) | async-done | bytes 1048592 | tf_op jit(solution)/shard_map/all_gather | solution.py:221
  188.2 7.3 %project.3 = bf16[6,128,128]{2,1,0:T(8,128)(2,1)} custom-call(bf16[128,4096]{1,0:T(8,128)(2,1)} %all-gather.9.cloned.1.call-done.x_ref, f32[1,4096]{1,0:T(1,128)} %get-tuple-element.10.gain_ref, bf16[2,4096,128]{2,1,0:T(8,128)(2,1)} %refs_0_.3, bf16[2,4096,128]{2,1,0:T(8,128)(2,1)} %refs_1_.3, bf16[2,4096,128]{2,1,0:T(8,128)(2,1)} %refs_2_.3, ...), custom_call_target="tpu_custom_call" | custom-call | tf_op jit(solution)/shard_map/project/pallas_call | solution.py:50
  195.4 1.1 copy.22
  196.5 9.0 %all_to_all.55 = bf16[6,128,128]{2,0,1:T(8,128)(2,1)S(1)} all-to-all(bf16[6,128,128]{2,0,1:T(8,128)(2,1)S(1)} %copy.22), channel_id=1, replica_groups=mesh['tp'=8,'dp'=4] {'dp'}, dimensions={1} | all-to-all | bytes 393216 | tf_op jit(solution)/shard_map/all_to_all | solution.py:213
  205.5 0.2 copy.29
  205.7 0.7 all_to_all.47.vec_ref
  206.4 12.4 %recur.3 = (f32[2,32,8,64,64]{4,3,2,1,0:T(8,128)}, bf16[32,512]{1,0:T(8,128)(2,1)}) custom-call(bf16[6,32,512]{2,1,0:T(8,128)(2,1)} %all_to_all.47.vec_ref, s32[32,128]{1,0:T(8,128)} %broadcast_in_dim.2.lens_ref, f32[1,512]{1,0:T(1,128)} %get-tuple-element.16.base_ref, f32[1,512]{1,0:T(1,128)} %get-tuple-element.19.rate_ref, ...), custom_call_target="tpu_custom_call", output_to_operand_aliasing={{0}: (6, {})} | custom-call | tf_op jit(solution)/shard_map/recur/pallas_call | solution.py:170
  218.9 6.1 %all_gather.26 = bf16[128,512]{1,0:T(8,128)(2,1)} all-gather(bf16[32,512]{1,0:T(8,128)(2,1)} %get-tuple-element.8), channel_id=1, replica_groups=mesh['tp'=8,'dp'=4] {'dp'}, dimensions={0}, use_global_device_ids=true | all-gather | bytes 163840 | tf_op jit(solution)/shard_map/all_gather | solution.py:217
  225.0 39.2 %all-gather.11.cloned.1.call-done.x_ref = bf16[128,4096]{1,0:T(8,128)(2,1)} async-done(((bf16[128,512]{1,0:T(8,128)(2,1)}), bf16[128,4096]{1,0:T(8,128)(2,1)}) %all-gather.11.cloned.1.call-update) | async-done | bytes 1048592 | tf_op jit(solution)/shard_map/all_gather | solution.py:218
  264.2 3.4 %fold.3 = bf16[128,128]{1,0:T(8,128)(2,1)} custom-call(bf16[128,4096]{1,0:T(8,128)(2,1)} %all-gather.11.cloned.1.call-done.x_ref, bf16[2,4096,128]{2,1,0:T(8,128)(2,1)} %w_ref.3), custom_call_target="tpu_custom_call" | custom-call | tf_op jit(solution)/shard_map/fold/pallas_call | solution.py:88
  267.6 7.2 %all_to_all.56 = bf16[4,32,128]{2,1,0:T(8,128)(2,1)S(1)} all-to-all(bf16[4,32,128]{2,1,0:T(8,128)(2,1)} %bitcast.19), channel_id=1, replica_groups=mesh['tp'=8,'dp'=4] {'dp'}, dimensions={0} | all-to-all | bytes 65536 | tf_op jit(solution)/shard_map/all_to_all | solution.py:222
  274.8 0.6 copy_bitcast_fusion.2
  (8 shorter events, 0.1 us)
Async XLA Ops:
  7.2 48.5 %all-gather.5.cloned.1.call-start = ((), (), s32[]{:S(2)}) async-start(), calls=%async_computation.3 | async-start | bytes 1179648 | tf_op jit(solution)/shard_map/all_gather | solution.py:208
  55.7 12.6 %copy-start = (f32[2,512]{1,0:T(2,128)S(1)}, f32[2,512]{1,0:T(2,128)}, u32[]{:S(2)}) copy-start(f32[2,512]{1,0:T(2,128)} %param.24) | copy-start | bytes 12292
  55.7 19.4 %copy-start.1 = (s32[32]{0:T(128)S(1)}, s32[32]{0:T(128)}, u32[]{:S(2)}) copy-start(s32[32]{0:T(128)} %param.15) | copy-start | bytes 388
  64.8 9.4 %all-to-all-start = ((bf16[6,128,128]{2,0,1:T(8,128)(2,1)}), bf16[6,128,128]{2,0,1:T(8,128)(2,1)S(1)}, u32[]{:S(2)}, u32[]{:S(2)}) async-start(bf16[6,128,128]{2,0,1:T(8,128)(2,1)} %copy.20), calls=%async_computation | async-start | bytes 524288 | tf_op jit(solution)/shard_map/all_to_all | solution.py:213
  68.2 65.0 %all-gather.7.cloned.1.call-start = ((), (), s32[]{:S(2)}) async-start(), calls=%async_computation.4 | async-start | bytes 1179648 | tf_op jit(solution)/shard_map/all_gather | solution.py:218
  94.3 93.9 %all-gather.9.cloned.1.call-start = ((), (), s32[]{:S(2)}) async-start(), calls=%async_computation.5 | async-start | bytes 1081344 | tf_op jit(solution)/shard_map/all_gather | solution.py:221
  136.6 127.6 %all-gather.11.cloned.1.call-start = ((), (), s32[]{:S(2)}) async-start(), calls=%async_computation.6 | async-start | bytes 1179648 | tf_op jit(solution)/shard_map/all_gather | solution.py:218
Sparse Core Ops, SparseCore 0:
  15.8 39.8 all-gather.4
  94.4 38.7 all-gather.6
  136.8 51.3 all-gather.8
  225.1 39.0 all-gather.10

commit v2 on v1

--- a/solution.py
+++ b/solution.py
@@ -13,7 +13,145 @@
 VMEM_LIMIT = 56 * 1024 * 1024
 
 
-def project_body(x_ref, gain_ref, *refs, features, steps):
+MESH = pl.DeviceIdType.MESH
+
+
+def greet(peers):
+    barrier = pltpu.get_barrier_semaphore()
+    for tp, dp in peers:
+        pl.semaphore_signal(barrier, inc=1, device_id=(tp, dp), device_id_type=MESH)
+    pl.semaphore_wait(barrier, len(peers))
+
+
+def gather_body(x_ref, out_ref, own_sem, send_sem, recv_sem, *, tp, dp):
+    t, d = lax.axis_index("tp"), lax.axis_index("dp")
+    core = lax.rem(d, 2)
+    sibling = d + 1 - 2 * core
+    others = [lax.rem(d + 2 * k, dp) for k in range(1, dp // 2)]
+    sent = []
+
+    def send(source, slot, to_t, to_d):
+        copy = pltpu.make_async_remote_copy(
+            src_ref=source,
+            dst_ref=out_ref.at[slot],
+            send_sem=send_sem.at[len(sent)],
+            recv_sem=recv_sem.at[slot],
+            device_id=(to_t, to_d),
+            device_id_type=MESH,
+        )
+        copy.start()
+        sent.append(copy)
+
+    def arrived(slot):
+        pltpu.make_async_remote_copy(
+            src_ref=x_ref,
+            dst_ref=out_ref.at[slot],
+            send_sem=send_sem.at[0],
+            recv_sem=recv_sem.at[slot],
+            device_id=(t, sibling),
+            device_id_type=MESH,
+        ).wait_recv()
+
+    rows = [lax.rem(t + k, tp) for k in range(1, tp)]
+    greet([(r, d) for r in rows] + [(t, o) for o in others] + [(t, sibling)])
+    mine = t * dp + d
+    own = pltpu.make_async_copy(x_ref, out_ref.at[mine], own_sem)
+    own.start()
+    for r in rows:
+        send(x_ref, mine, r, d)
+    for o in others + [sibling]:
+        send(x_ref, mine, t, o)
+    for k in range(1, tp):
+        slot = lax.rem(t + tp - k, tp) * dp + d
+        arrived(slot)
+        for o in others + [sibling]:
+            send(out_ref.at[slot], slot, t, o)
+    for k in range(tp):
+        for o in others:
+            slot = lax.rem(t + tp - k, tp) * dp + o
+            arrived(slot)
+            send(out_ref.at[slot], slot, t, sibling)
+    for k in range(tp):
+        for o in [d] + others:
+            arrived(lax.rem(t + tp - k, tp) * dp + o + sibling - d)
+    own.wait()
+    for copy in sent:
+        copy.wait_send()
+
+
+def gather(x, tp, dp, number):
+    count = (tp - 1) + tp * (dp // 2) + tp * (dp // 2 - 1)
+    return pl.pallas_call(
+        functools.partial(gather_body, tp=tp, dp=dp),
+        out_shape=jax.ShapeDtypeStruct((tp * dp,) + x.shape, x.dtype),
+        in_specs=[pl.BlockSpec(memory_space=pltpu.VMEM)],
+        out_specs=pl.BlockSpec(memory_space=pltpu.VMEM),
+        scratch_shapes=[
+            pltpu.SemaphoreType.DMA,
+            pltpu.SemaphoreType.DMA((count,)),
+            pltpu.SemaphoreType.DMA((tp * dp,)),
+        ],
+        compiler_params=pltpu.CompilerParams(collective_id=number, has_side_effects=True),
+        name="gather",
+    )(x)
+
+
+def exchange_body(x_ref, out_ref, own_sem, send_sem, recv_sem, *, dp):
+    t, d = lax.axis_index("tp"), lax.axis_index("dp")
+    peers = [lax.rem(d + k, dp) for k in range(1, dp)]
+    greet([(t, o) for o in peers])
+    own = pltpu.make_async_copy(x_ref.at[d], out_ref.at[d], own_sem)
+    own.start()
+    sent = []
+    for k, o in enumerate(peers):
+        copy = pltpu.make_async_remote_copy(
+            src_ref=x_ref.at[o],
+            dst_ref=out_ref.at[d],
+            send_sem=send_sem.at[k],
+            recv_sem=recv_sem.at[k],
+            device_id=(t, o),
+            device_id_type=MESH,
+        )
+        copy.start()
+        sent.append(copy)
+    for k in range(1, dp):
+        source = lax.rem(d + dp - k, dp)
+        pltpu.make_async_remote_copy(
+            src_ref=x_ref.at[source],
+            dst_ref=out_ref.at[source],
+            send_sem=send_sem.at[k - 1],
+            recv_sem=recv_sem.at[k - 1],
+            device_id=(t, source),
+            device_id_type=MESH,
+        ).wait_recv()
+    own.wait()
+    for copy in sent:
+        copy.wait_send()
+
+
+def exchange(x, dp, number):
+    return pl.pallas_call(
+        functools.partial(exchange_body, dp=dp),
+        out_shape=jax.ShapeDtypeStruct(x.shape, x.dtype),
+        in_specs=[pl.BlockSpec(memory_space=pltpu.VMEM)],
+        out_specs=pl.BlockSpec(memory_space=pltpu.VMEM),
+        scratch_shapes=[
+            pltpu.SemaphoreType.DMA,
+            pltpu.SemaphoreType.DMA((dp - 1,)),
+            pltpu.SemaphoreType.DMA((dp - 1,)),
+        ],
+        compiler_params=pltpu.CompilerParams(collective_id=number, has_side_effects=True),
+        name="exchange",
+    )(x)
+
+
+def joined_block(x_ref, across):
+    if across:
+        return jnp.concatenate([x_ref[j] for j in range(x_ref.shape[0])], axis=1)
+    return x_ref[...].reshape(x_ref.shape[0] * x_ref.shape[1], x_ref.shape[2])
+
+
+def project_body(x_ref, gain_ref, *refs, features, steps, across):
     weights, out_ref, acc, square = refs[:6], refs[6], refs[7], refs[8]
     step = pl.program_id(0)
     slim = weights[0].shape[-1]
@@ -23,7 +161,7 @@
         acc[...] = jnp.zeros_like(acc)
         square[...] = jnp.zeros_like(square)
 
-    values = x_ref[...].astype(jnp.float32)
+    values = joined_block(x_ref, across).astype(jnp.float32)
     square[...] += jnp.sum(values * values, axis=1, keepdims=True)
     scaled = (values * gain_ref[...]).astype(jnp.bfloat16)
     if slim % 128 == 0:
@@ -39,24 +177,27 @@
     def _():
         factor = lax.rsqrt(square[...] / features + RMS_EPS)
         for idx in range(6):
-            out_ref[idx] = (acc[idx] * factor).astype(out_ref.dtype)
-
-
-def project(x, gain, weights, layer):
-    rows, features = x.shape
-    slim = weights[0].shape[2]
-    depth = 512
-    steps = features // depth
-    return pl.pallas_call(
-        functools.partial(project_body, features=features, steps=steps),
+            done = (acc[idx] * factor).astype(out_ref.dtype)
+            share = out_ref.shape[2]
+            for j in range(out_ref.shape[0]):
+                out_ref[j, idx] = done[j * share : (j + 1) * share]
+
+
+def project(x, gain, weights, layer, steps, dp, across):
+    features, slim = weights[0].shape[1:]
+    part = x.shape[0] // steps
+    depth = features // steps
+    rows = x.shape[1] * (1 if across else part)
+    return pl.pallas_call(
+        functools.partial(project_body, features=features, steps=steps, across=across),
         grid=(steps,),
-        out_shape=jax.ShapeDtypeStruct((6, rows, slim), jnp.bfloat16),
+        out_shape=jax.ShapeDtypeStruct((dp, 6, rows // dp, slim), jnp.bfloat16),
         in_specs=[
-            pl.BlockSpec((rows, depth), lambda i: (0, i)),
+            pl.BlockSpec((part,) + x.shape[1:], lambda i: (i, 0, 0)),
             pl.BlockSpec((1, depth), lambda i: (0, i)),
         ]
         + [pl.BlockSpec((1, depth, slim), lambda i: (layer, i, 0))] * 6,
-        out_specs=pl.BlockSpec((6, rows, slim), lambda i: (0, 0, 0)),
+        out_specs=pl.BlockSpec((dp, 6, rows // dp, slim), lambda i: (0, 0, 0, 0)),
         scratch_shapes=[
             pltpu.VMEM((6, rows, slim), jnp.float32),
             pltpu.VMEM((rows, 1), jnp.float32),
@@ -73,24 +214,24 @@
     def _():
         acc[...] = jnp.zeros_like(acc)
 
-    acc[...] += jnp.dot(x_ref[...], w_ref[0], preferred_element_type=jnp.float32)
+    acc[...] += jnp.dot(joined_block(x_ref, False), w_ref[0], preferred_element_type=jnp.float32)
 
     @pl.when(step == steps - 1)
     def _():
         out_ref[...] = acc[...].astype(out_ref.dtype)
 
 
-def fold(x, weight, layer):
-    rows, features = x.shape
-    slim = weight.shape[2]
-    depth = 1024
-    steps = features // depth
+def fold(x, weight, layer, steps):
+    features, slim = weight.shape[1:]
+    part = x.shape[0] // steps
+    depth = features // steps
+    rows = part * x.shape[1]
     return pl.pallas_call(
         functools.partial(fold_body, steps=steps),
         grid=(steps,),
         out_shape=jax.ShapeDtypeStruct((rows, slim), jnp.bfloat16),
         in_specs=[
-            pl.BlockSpec((rows, depth), lambda i: (0, i)),
+            pl.BlockSpec((part,) + x.shape[1:], lambda i: (i, 0, 0)),
             pl.BlockSpec((1, depth, slim), lambda i: (layer, i, 0)),
         ],
         out_specs=pl.BlockSpec((rows, slim), lambda i: (0, 0)),
@@ -203,24 +344,29 @@
     state,
 ):
     weights = (w_recept, w_key, w_value, w_decay, w_rate, w_gate)
-    lens = jnp.broadcast_to(lengths[:, None], (lengths.shape[0], 128))
-    every = lax.all_gather(tokens, "dp", axis=0, tiled=True)
-    every = lax.all_gather(every, "tp", axis=1, tiled=True)
+    tp, dp = lax.axis_size("tp"), lax.axis_size("dp")
+    rows, slim = lengths.shape[0], w_out.shape[2]
+    lens = jnp.broadcast_to(lengths[:, None], (rows, 128))
+    every, across = gather(tokens, tp, dp, 0), False
     states = None
     for layer in range(2):
         pick = slice(layer, layer + 1)
-        pieces = project(every, norm_gain[pick], weights, layer)
-        vec = lax.all_to_all(pieces, "dp", split_axis=1, concat_axis=2, tiled=True)
+        pieces = project(every, norm_gain[pick], weights, layer, tp, dp, across)
+        vec = exchange(pieces, dp, 1 + layer)
+        vec = vec.transpose(1, 2, 0, 3).reshape(6, rows, dp * slim)
         states, mixed = recur(
             vec, lens, decay_base[pick], rate_base[pick], group_gain[pick], state, states, layer
         )
-        rows_all = lax.all_gather(mixed, "dp", axis=0, tiled=True)
-        rows_all = lax.all_gather(rows_all, "tp", axis=1, tiled=True)
-        columns = fold(rows_all, w_out, layer)
+        columns = fold(gather(mixed, tp, dp, 3 + layer), w_out, layer, tp)
         if layer == 0:
-            every = lax.all_gather(columns, ("tp", "dp"), axis=1, tiled=True)
-    current = lax.all_to_all(columns, "dp", split_axis=0, concat_axis=1, tiled=True)
-    return (current, states)
+            across = slim % 128 == 0
+            if across:
+                every = gather(columns, tp, dp, 5)
+            else:
+                every = lax.all_gather(columns, ("tp", "dp"), axis=1, tiled=True)
+                every = every.reshape(dp * rows, tp, dp * slim).transpose(1, 0, 2)
+    current = exchange(columns.reshape(dp, rows, slim), dp, 6)
+    return (current.transpose(1, 0, 2).reshape(rows, dp * slim), states)
 
 
 def solution(mesh):

time: 283 us -> 153 us (0.54)
  waiting for transfers between devices: 172 us -> 0 us
  Pallas kernels: 46.3 us -> 141 us
  blocking collectives: 36.7 us -> 0 us
  between operations: 13.8 us -> 0.69 us
  starting transfers between devices: 3.57 us -> 0 us
    all_gather x4 -> x0, waiting for transfers between devices: 167 us -> none  [the longest x2 78.1 us: on_device(): rows_all = lax.all_gather(rows_all, 'tp', axis=1, tiled=True)]
    pallas_call x0 -> x7, Pallas kernels: none -> 90.9 us  [the longest x4 73.2 us: gather(): pl.pallas_call(functools.partial(gather_body, tp=tp, dp=dp), out_shape=ja...]
    all_gather x3 -> x0, blocking collectives: 20.5 us -> none  [the longest x2 12.1 us: on_device(): rows_all = lax.all_gather(mixed, 'dp', axis=0, tiled=True)]
    all_to_all x2 -> x0, blocking collectives: 16.2 us -> none  [the longest x1 9.01 us: on_device(): vec = lax.all_to_all(pieces, 'dp', split_axis=1, concat_axis=2, tiled=True)]
    all_to_all x1 -> x0, waiting for transfers between devices: 5.31 us -> none  [on_device(): vec = lax.all_to_all(pieces, 'dp', split_axis=1, concat_axis=2, tiled=True)]
    reshape x0 -> x3, local copies, waits for them, and re-layouts: none -> 4.63 us  [the longest x2 3.25 us: on_device(): vec = vec.transpose(1, 2, 0, 3).reshape(6, rows, dp * slim)]
    pallas_call x2, Pallas kernels: 6.84 us -> 11.1 us  [fold(): pl.pallas_call(functools.partial(fold_body, steps=steps), grid=(steps,),...]
    all_to_all x1 -> x0, starting transfers between devices: 3.41 us -> none  [on_device(): vec = lax.all_to_all(pieces, 'dp', split_axis=1, concat_axis=2, tiled=True)]
  transfers between devices with their start and end apart: 5 -> 0, of which waited for: 5 -> 0; matrix products, arithmetic and copies ran while one was open for 1% -> 0% of each run, Pallas kernels for 0% -> 0%
where the time goes in v2:
time: 153 us; the launch traced here: 152 us
  Pallas kernels  141 us (92%)
  local copies, waits for them, and re-layouts  10.2 us (7%)
    pallas_call x4, Pallas kernels, gather(): pl.pallas_call(functools.partial(gather_body, tp=tp, dp=dp), out_shape=ja...  73.2 us
    pallas_call x2, Pallas kernels, recur(): pl.pallas_call(recur_body, grid=(rows // group,), out_shape=(jax.ShapeDty...  24.9 us
    pallas_call x3, Pallas kernels, exchange(): pl.pallas_call(functools.partial(exchange_body, dp=dp), out_shape=jax.Sha...  17.6 us
    pallas_call x2, Pallas kernels, project(): pl.pallas_call(functools.partial(project_body, features=features, steps=s...  14.5 us
    pallas_call x2, Pallas kernels, fold(): pl.pallas_call(functools.partial(fold_body, steps=steps), grid=(steps,),...  11.1 us
    reshape x2, local copies, waits for them, and re-layouts, on_device(): vec = vec.transpose(1, 2, 0, 3).reshape(6, rows, dp * slim)  3.25 us

profile of v2, /device:TPU:0, one launch (start us, length us, event | category | flops | bytes accessed | tf_op | source)
XLA Modules:
  0.0 152.2 jit_solution(565506755134644324)
XLA Ops:
  0.6 1.4 fusion.3
  2.0 1.4 fusion.1
  3.4 1.3 broadcast_in_dim.2.lens_ref
  4.7 1.5 fusion
  6.2 19.4 %gather.4.x_ref = bf16[32,32,512]{2,1,0:T(8,128)(2,1)} custom-call(bf16[32,512]{1,0:T(8,128)(2,1)} %x_ref.1), custom_call_target="tpu_custom_call" | custom-call | tf_op jit(solution)/shard_map/gather/pallas_call | solution.py:84
  25.5 7.3 %project.2.x_ref = bf16[4,6,32,128]{3,2,1,0:T(8,128)(2,1)} custom-call(bf16[32,32,512]{2,1,0:T(8,128)(2,1)} %gather.4.x_ref, f32[1,4096]{1,0:T(1,128)} %get-tuple-element.11.gain_ref, bf16[2,4096,128]{2,1,0:T(8,128)(2,1)} %refs_0_.3, bf16[2,4096,128]{2,1,0:T(8,128)(2,1)} %refs_1_.3, bf16[2,4096,128]{2,1,0:T(8,128)(2,1)} %refs_2_.3, ...), custom_call_target="tpu_custom_call" | custom-call | tf_op jit(solution)/shard_map/project/pallas_call | solution.py:191
  32.8 6.3 %exchange.3 = bf16[4,6,32,128]{3,2,1,0:T(8,128)(2,1)} custom-call(bf16[4,6,32,128]{3,2,1,0:T(8,128)(2,1)} %project.2.x_ref), custom_call_target="tpu_custom_call" | custom-call | tf_op jit(solution)/shard_map/exchange/pallas_call | solution.py:133
  39.1 1.6 %copy_bitcast_fusion.1.vec_ref = bf16[6,32,512]{2,1,0:T(8,128)(2,1)} fusion(bf16[4,6,32,128]{3,2,1,0:T(8,128)(2,1)} %exchange.3), kind=kLoop, calls=%fused_computation.1 | loop fusion | bytes 393216 | tf_op jit(solution)/shard_map/reshape | solution.py:356
  40.8 12.4 %recur.2 = (f32[2,32,8,64,64]{4,3,2,1,0:T(8,128)}, bf16[32,512]{1,0:T(8,128)(2,1)}) custom-call(bf16[6,32,512]{2,1,0:T(8,128)(2,1)} %copy_bitcast_fusion.1.vec_ref, s32[32,128]{1,0:T(8,128)} %broadcast_in_dim.2.lens_ref, f32[1,512]{1,0:T(1,128)} %get-tuple-element.17.base_ref, f32[1,512]{1,0:T(1,128)} %get-tuple-element.18.rate_ref, ...), custom_call_target="tpu_custom_call" | custom-call | tf_op jit(solution)/shard_map/recur/pallas_call | solution.py:311
  53.2 17.1 %gather.5.x_ref = bf16[32,32,512]{2,1,0:T(8,128)(2,1)} custom-call(bf16[32,512]{1,0:T(8,128)(2,1)} %get-tuple-element.6.x_ref), custom_call_target="tpu_custom_call" | custom-call | tf_op jit(solution)/shard_map/gather/pallas_call | solution.py:84
  70.3 5.5 %fold.2.x_ref = bf16[128,128]{1,0:T(8,128)(2,1)} custom-call(bf16[32,32,512]{2,1,0:T(8,128)(2,1)} %gather.5.x_ref, bf16[2,4096,128]{2,1,0:T(8,128)(2,1)} %w_ref.3), custom_call_target="tpu_custom_call" | custom-call | tf_op jit(solution)/shard_map/fold/pallas_call | solution.py:229
  75.8 19.2 %gather.6.x_ref = bf16[32,128,128]{2,1,0:T(8,128)(2,1)} custom-call(bf16[128,128]{1,0:T(8,128)(2,1)} %fold.2.x_ref), custom_call_target="tpu_custom_call" | custom-call | tf_op jit(solution)/shard_map/gather/pallas_call | solution.py:84
  95.1 7.2 %project.3.x_ref = bf16[4,6,32,128]{3,2,1,0:T(8,128)(2,1)} custom-call(bf16[32,128,128]{2,1,0:T(8,128)(2,1)} %gather.6.x_ref, f32[1,4096]{1,0:T(1,128)} %get-tuple-element.10.gain_ref, bf16[2,4096,128]{2,1,0:T(8,128)(2,1)} %refs_0_.3, bf16[2,4096,128]{2,1,0:T(8,128)(2,1)} %refs_1_.3, bf16[2,4096,128]{2,1,0:T(8,128)(2,1)} %refs_2_.3, ...), custom_call_target="tpu_custom_call" | custom-call | tf_op jit(solution)/shard_map/project/pallas_call | solution.py:191
  102.3 6.3 %exchange.4 = bf16[4,6,32,128]{3,2,1,0:T(8,128)(2,1)} custom-call(bf16[4,6,32,128]{3,2,1,0:T(8,128)(2,1)} %project.3.x_ref), custom_call_target="tpu_custom_call" | custom-call | tf_op jit(solution)/shard_map/exchange/pallas_call | solution.py:133
  108.6 1.6 %copy_bitcast_fusion.vec_ref = bf16[6,32,512]{2,1,0:T(8,128)(2,1)} fusion(bf16[4,6,32,128]{3,2,1,0:T(8,128)(2,1)} %exchange.4), kind=kLoop, calls=%fused_computation | loop fusion | bytes 393216 | tf_op jit(solution)/shard_map/reshape | solution.py:356
  110.2 12.4 %recur.3 = (f32[2,32,8,64,64]{4,3,2,1,0:T(8,128)}, bf16[32,512]{1,0:T(8,128)(2,1)}) custom-call(bf16[6,32,512]{2,1,0:T(8,128)(2,1)} %copy_bitcast_fusion.vec_ref, s32[32,128]{1,0:T(8,128)} %broadcast_in_dim.2.lens_ref, f32[1,512]{1,0:T(1,128)} %get-tuple-element.16.base_ref, f32[1,512]{1,0:T(1,128)} %get-tuple-element.19.rate_ref, ...), custom_call_target="tpu_custom_call", output_to_operand_aliasing={{0}: (6, {})} | custom-call | tf_op jit(solution)/shard_map/recur/pallas_call | solution.py:311
  122.6 17.6 %gather.7.x_ref = bf16[32,32,512]{2,1,0:T(8,128)(2,1)} custom-call(bf16[32,512]{1,0:T(8,128)(2,1)} %get-tuple-element.8.x_ref), custom_call_target="tpu_custom_call" | custom-call | tf_op jit(solution)/shard_map/gather/pallas_call | solution.py:84
  140.2 5.5 %fold.3 = bf16[128,128]{1,0:T(8,128)(2,1)} custom-call(bf16[32,32,512]{2,1,0:T(8,128)(2,1)} %gather.7.x_ref, bf16[2,4096,128]{2,1,0:T(8,128)(2,1)} %w_ref.3), custom_call_target="tpu_custom_call" | custom-call | tf_op jit(solution)/shard_map/fold/pallas_call | solution.py:229
  145.8 5.1 %exchange.5 = bf16[4,32,128]{2,1,0:T(8,128)(2,1)} custom-call(bf16[4,32,128]{2,1,0:T(8,128)(2,1)} %bitcast.19), custom_call_target="tpu_custom_call" | custom-call | tf_op jit(solution)/shard_map/exchange/pallas_call | solution.py:133
  150.8 1.4 copy_bitcast_fusion.2
